TPU v7x, 32 devices: a whole 2x2x4 slice. The times are simulated.
32 devices in a mesh: fs: 8 (over z, y), tp: 4 (over x, core).
Axes of the slice: x: 2, y: 2, z: 4, core: 2. Of those that a mesh axis runs over, the one named last changes fastest.
Arguments:
- tokens: bfloat16 [6144, 2048], P('fs', 'tp'), may hold values from -40 to 40
- gain_one: float32 [2048], P('tp'), may hold values from 0.1 to 1.9
- w_gate: float32 [2048, 3072], P('fs', 'tp'), may hold values from -0.125 to 0.125
- w_up: float32 [2048, 3072], P('fs', 'tp'), may hold values from -0.125 to 0.125
- w_down: float32 [3072, 2048], P('tp', 'fs'), may hold values from -0.109375 to 0.109375
- scale_gate: float32 [3072], P('tp'), may hold values from 0.5 to 2
- scale_up: float32 [3072], P('tp'), may hold values from 0.5 to 2
- scale_down: float32 [2048], P('tp'), may hold values from 0.5 to 2
- gain_mix: float32 [2048], P('tp'), may hold values from 0.1 to 1.9
- w_query: float32 [2048, 2048], P('fs', 'tp'), may hold values from -0.125 to 0.125
- w_key: float32 [2048, 2048], P('fs', 'tp'), may hold values from -0.125 to 0.125
- w_value: float32 [2048, 2048], P('fs', 'tp'), may hold values from -0.125 to 0.125
- w_outgate: float32 [2048, 2048], P('fs', 'tp'), may hold values from -0.125 to 0.125
- scale_query: float32 [2048], P('tp'), may hold values from 0.5 to 2
- scale_key: float32 [2048], P('tp'), may hold values from 0.5 to 2
- scale_value: float32 [2048], P('tp'), may hold values from 0.5 to 2
- scale_outgate: float32 [2048], P('tp'), may hold values from 0.5 to 2
- ret_gain: float32 [2048], P('tp'), may hold values from 0.1 to 1.9
- decay_rate: float32 [8], P('tp'), may hold values from 0 to 2
- w_mix: float32 [2048, 2048], P('tp', 'fs'), may hold values from -0.125 to 0.125
- scale_mix: float32 [2048], P('tp'), may hold values from 0.5 to 2
- gain_two: float32 [2048], P('tp'), may hold values from 0.1 to 1.9
Outputs:
- layer_out: bfloat16 [6144, 2048], P('fs', 'tp')
All inputs are finite; a program needn't handle non-finite values.
Results may differ from a plain program's by a relative error of at most 0.022.
Values may be sent and summed in bfloat16 or wider, within the bound.
A program may use at most 128 MiB of HBM per device.

v0:
```python
import jax
import jax.numpy as jnp
from jax import lax
from jax.sharding import PartitionSpec as P

D = 2048
LEN = 256
BLK = 128
EPS = 1e-06
HEAD_EPS = 0.1


def rotate_pairs(values):
    paired = values.reshape(values.shape[:-1] + (values.shape[-1] // 2, 2))
    return jnp.stack((-paired[..., 1], paired[..., 0]), axis=-1).reshape(values.shape)


def retain(query_rows, key_rows, value_rows, decay_rate, length, block):
    highest = lax.Precision.HIGHEST
    total_rows = query_rows.shape[0]
    heads = decay_rate.shape[0]
    head_size = query_rows.shape[1] // heads
    sequences = total_rows // length
    nblocks = length // block

    def split_heads(values):
        return values.astype(jnp.float32).reshape(sequences, length, heads, head_size)

    freq = 1.0 / 10000.0 ** jnp.linspace(0.0, 1.0, head_size // 2, dtype=jnp.float32)
    freq = jnp.repeat(freq, 2)
    angles = jnp.arange(length, dtype=jnp.float32)[:, None] * freq[None, :]
    sines = jnp.sin(angles)[None, :, None, :]
    cosines = jnp.cos(angles)[None, :, None, :]
    queries = split_heads(query_rows)
    queries = queries * cosines + rotate_pairs(queries) * sines
    keys_all = split_heads(key_rows) * head_size ** (-0.5)
    keys_all = keys_all * cosines + rotate_pairs(keys_all) * sines
    values_all = split_heads(value_rows)
    log_decay = -decay_rate
    offsets = jnp.arange(block, dtype=jnp.float32)
    distance = offsets[:, None] - offsets[None, :]
    inside = jnp.where(
        distance >= 0, jnp.exp(log_decay[:, None, None] * jnp.maximum(distance, 0.0)), 0.0
    )
    query_decay = jnp.exp(log_decay[None, :] * (offsets[:, None] + 1.0))
    key_decay = jnp.exp(log_decay[None, :] * (block - 1.0 - offsets[:, None]))
    block_decay = jnp.exp(log_decay * block)

    def to_blocks(values):
        return jnp.moveaxis(values.reshape(sequences, nblocks, block, heads, head_size), 1, 0)

    def advance(carried, pieces):
        query_blk, key_blk, value_blk = pieces
        scores = jnp.einsum("snhd,smhd->shnm", query_blk, key_blk, precision=highest) * inside
        within = jnp.einsum("shnm,smhe->snhe", scores, value_blk, precision=highest)
        across = (
            jnp.einsum("snhd,shde->snhe", query_blk, carried, precision=highest)
            * query_decay[None, :, :, None]
        )
        weighted = key_blk * key_decay[None, :, :, None]
        carried = carried * block_decay[None, :, None, None] + jnp.einsum(
            "smhd,smhe->shde", weighted, value_blk, precision=highest
        )
        return (carried, within + across)

    initial = jnp.zeros((sequences, heads, head_size, head_size), jnp.float32)
    _, results = lax.scan(
        advance, initial, (to_blocks(queries), to_blocks(keys_all), to_blocks(values_all))
    )
    results = jnp.moveaxis(results, 0, 1).reshape(sequences, length, heads, head_size)
    results = results * lax.rsqrt(jnp.mean(results * results, axis=-1, keepdims=True) + HEAD_EPS)
    return results.reshape(total_rows, heads * head_size)


def normed_rows(hidden_in, norm_gain):
    widened = hidden_in.astype(jnp.float32)
    totals = lax.psum(jnp.sum(widened * widened, axis=1), "tp")
    scaled = widened * lax.rsqrt(totals / D + EPS)[:, None] * norm_gain
    return lax.all_gather(scaled.astype(jnp.bfloat16), "tp", axis=1, tiled=True)


def summed_share(partial_value):
    rounded = lax.optimization_barrier(partial_value.astype(jnp.bfloat16))
    return lax.psum_scatter(
        rounded.astype(jnp.float32).astype(jnp.bfloat16), "tp", scatter_dimension=1, tiled=True
    ).astype(jnp.float32)


def ffn_gathered(features, gate_low, up_low, down_low, scale_gate, scale_up):
    gate_add = jnp.dot(
        features,
        lax.all_gather(gate_low, "fs", axis=0, tiled=True),
        preferred_element_type=jnp.float32,
    )
    up_add = jnp.dot(
        features,
        lax.all_gather(up_low, "fs", axis=0, tiled=True),
        preferred_element_type=jnp.float32,
    )
    hidden = (jax.nn.silu(gate_add * scale_gate) * (up_add * scale_up)).astype(jnp.bfloat16)
    return jnp.dot(
        hidden,
        lax.all_gather(down_low, "fs", axis=1, tiled=True),
        preferred_element_type=jnp.float32,
    )


def per_device(
    tokens,
    gain_one,
    w_gate,
    w_up,
    w_down,
    scale_gate,
    scale_up,
    scale_down,
    gain_mix,
    w_query,
    w_key,
    w_value,
    w_outgate,
    scale_query,
    scale_key,
    scale_value,
    scale_outgate,
    ret_gain,
    decay_rate,
    w_mix,
    scale_mix,
    gain_two,
):
    norm_one, norm_mix, norm_two, down_cols, mix_cols = (
        gain_one,
        gain_mix,
        gain_two,
        scale_down,
        scale_mix,
    )
    gate_low = w_gate.astype(jnp.bfloat16)
    up_low = w_up.astype(jnp.bfloat16)
    down_low = w_down.astype(jnp.bfloat16)
    ffn_one = ffn_gathered(
        normed_rows(tokens, norm_one), gate_low, up_low, down_low, scale_gate, scale_up
    )
    first = (tokens.astype(jnp.float32) + 0.5 * summed_share(ffn_one) * down_cols).astype(
        jnp.bfloat16
    )
    features = normed_rows(first, norm_mix)
    pieces = (
        lax.all_gather(w_query.astype(jnp.bfloat16), "fs", axis=0, tiled=True),
        lax.all_gather(w_key.astype(jnp.bfloat16), "fs", axis=0, tiled=True),
        lax.all_gather(w_value.astype(jnp.bfloat16), "fs", axis=0, tiled=True),
        lax.all_gather(w_outgate.astype(jnp.bfloat16), "fs", axis=0, tiled=True),
    )
    query_pre, key_pre, value_pre, outgate_pre = tuple(
        (jnp.dot(features, piece, preferred_element_type=jnp.float32) for piece in pieces)
    )
    query_rows = (query_pre * scale_query).astype(jnp.bfloat16)
    key_rows = (key_pre * scale_key).astype(jnp.bfloat16)
    value_rows = (value_pre * scale_value).astype(jnp.bfloat16)
    outgate_rows = (outgate_pre * scale_outgate).astype(jnp.bfloat16)
    retained = retain(query_rows, key_rows, value_rows, decay_rate, LEN, BLK)
    mixed = (retained * ret_gain * jax.nn.silu(outgate_rows.astype(jnp.float32))).astype(
        jnp.bfloat16
    )
    mix_partial = jnp.dot(
        mixed,
        lax.all_gather(w_mix.astype(jnp.bfloat16), "fs", axis=1, tiled=True),
        preferred_element_type=jnp.float32,
    )
    second = (first.astype(jnp.float32) + summed_share(mix_partial) * mix_cols).astype(jnp.bfloat16)
    ffn_two = ffn_gathered(
        normed_rows(second, norm_two), gate_low, up_low, down_low, scale_gate, scale_up
    )
    result = (second.astype(jnp.float32) + 0.5 * summed_share(ffn_two) * down_cols).astype(
        jnp.bfloat16
    )
    return result


def solution(mesh):
    return jax.shard_map(
        per_device,
        mesh=mesh,
        in_specs=(
            P("fs", "tp"),
            P("tp"),
            P("fs", "tp"),
            P("fs", "tp"),
            P("tp", "fs"),
            P("tp"),
            P("tp"),
            P("tp"),
            P("tp"),
            P("fs", "tp"),
            P("fs", "tp"),
            P("fs", "tp"),
            P("fs", "tp"),
            P("tp"),
            P("tp"),
            P("tp"),
            P("tp"),
            P("tp"),
            P("tp"),
            P("tp", "fs"),
            P("tp"),
            P("tp"),
        ),
        out_specs=P("fs", "tp"),
        check_vma=False,
    )
```

profile of v0, /device:TPU:0, one launch (start us, length us, event | category | flops | bytes accessed | tf_op | source)
XLA Modules:
  0.0 710.8 jit_solution(11164169633599705700)
XLA Ops:
  8.0 8.4 %psum.21 = f32[768]{0:T(1024)S(1)} all-reduce(f32[768]{0:T(1024)S(1)} %fusion.31), channel_id=1, replica_groups=mesh['fs'=8,'tp'=4] {'tp'}, use_global_device_ids=true, to_apply=%region_1.0 | all-reduce | flops 768 | bytes 6144 | tf_op jit(solution)/shard_map/psum | solution.py:77
  21.7 26.0 %all-gather.12.cloned.1.call-done = bf16[768,2048]{1,0:T(8,128)(2,1)} async-done(((bf16[768,512]{1,0:T(8,128)(2,1)}), bf16[768,2048]{1,0:T(8,128)(2,1)}) %all-gather.12.cloned.1.call-update) | async-done | bytes 3145744 | tf_op jit(solution)/shard_map/all_gather | solution.py:79
  47.6 62.2 %all-gather.14.cloned.1.call-done = bf16[2048,768]{1,0:T(8,128)(2,1)} async-done(((bf16[256,768]{1,0:T(8,128)(2,1)}), bf16[2048,768]{1,0:T(8,128)(2,1)}) %all-gather.14.cloned.1.call-update) | async-done | bytes 3145744 | tf_op jit(solution)/shard_map/all_gather | solution.py:92
  109.9 6.8 fusion.60
  116.7 54.1 %all-gather.16.cloned.1.call-done = bf16[2048,768]{1,0:T(8,128)(2,1)} async-done(((bf16[256,768]{1,0:T(8,128)(2,1)}), bf16[2048,768]{1,0:T(8,128)(2,1)}) %all-gather.16.cloned.1.call-update) | async-done | bytes 3145744 | tf_op jit(solution)/shard_map/all_gather | solution.py:97
  170.8 63.2 %all-gather.18.cloned.1.call-done = bf16[768,2048]{1,0:T(8,128)(2,1)} async-done(((bf16[768,256]{1,0:T(8,128)(2,1)}), bf16[768,2048]{1,0:T(8,128)(2,1)}) %all-gather.18.cloned.1.call-update) | async-done | bytes 3145744 | tf_op jit(solution)/shard_map/all_gather | solution.py:103
  234.0 11.0 %convolution_convert_fusion.2 = bf16[768,2048]{1,0:T(8,128)(2,1)} fusion(bf16[768,2048]{1,0:T(8,128)(2,1)} %all-gather.18.cloned.1.call-done, f32[768,768]{1,0:T(8,128)} %fusion.60, bf16[768,2048]{1,0:T(8,128)(2,1)S(1)} %copy-done.28, bf16[2048,768]{1,0:T(8,128)(2,1)} %all-gather.16.cloned.1.call-done, f32[768]{0:T(1024)S(1)} %copy-done.29, ...), kind=kOutput, calls=%fused_computation.31 | convolution fusion | flops 4838129664 | bytes 14948352 | tf_op jit(solution)/shard_map/dot_general | solution.py:101
  246.9 34.2 %reduce-scatter.4.cloned.1.call-done = bf16[768,512]{1,0:T(8,128)(2,1)} async-done(((bf16[768,2048]{1,0:T(8,128)(2,1)}), bf16[768,512]{1,0:T(8,128)(2,1)}) %reduce-scatter.4.cloned.1.call-update) | async-done | bytes 786448 | tf_op jit(solution)/shard_map/reduce_scatter | solution.py:84
  282.7 5.9 psum.22
  295.2 8.3 %multiply_cosine_fusion = (f32[2,128,256]{1,0,2:T(2,128)S(1)}, f32[2,128,256]{1,0,2:T(2,128)}, f32[2,128,256]{1,0,2:T(2,128)}) fusion(f32[2,128]{1,0:T(2,128)S(1)} %multiply_add_fusion.1, f32[256]{0:T(256)S(1)} %mul.404), kind=kLoop, calls=%fused_computation.82 | loop fusion | flops 327680 | bytes 788480 | tf_op jit(solution)/shard_map/cos | solution.py:33
  303.5 28.7 %all-gather.26.cloned.1.call-done = bf16[2048,512]{1,0:T(8,128)(2,1)} async-done(((bf16[256,512]{1,0:T(8,128)(2,1)}), bf16[2048,512]{1,0:T(8,128)(2,1)}) %all-gather.26.cloned.1.call-update) | async-done | bytes 2097168 | tf_op jit(solution)/shard_map/all_gather | solution.py:150
  332.2 28.6 %all-gather.20.cloned.1.call-done = bf16[768,2048]{1,0:T(8,128)(2,1)} async-done(((bf16[768,512]{1,0:T(8,128)(2,1)}), bf16[768,2048]{1,0:T(8,128)(2,1)}) %all-gather.20.cloned.1.call-update) | async-done | bytes 3145744 | tf_op jit(solution)/shard_map/all_gather | solution.py:79
  369.1 43.0 %all-gather.22.cloned.1.call-done = bf16[2048,512]{1,0:T(8,128)(2,1)} async-done(((bf16[256,512]{1,0:T(8,128)(2,1)}), bf16[2048,512]{1,0:T(8,128)(2,1)}) %all-gather.22.cloned.1.call-update) | async-done | bytes 2097168 | tf_op jit(solution)/shard_map/all_gather | solution.py:151
  412.1 6.0 broadcast_multiply_fusion
  453.1 8.8 %all-gather.24.cloned.1.call-done = bf16[2048,512]{1,0:T(8,128)(2,1)} async-done(((bf16[256,512]{1,0:T(8,128)(2,1)}), bf16[2048,512]{1,0:T(8,128)(2,1)}) %all-gather.24.cloned.1.call-update) | async-done | bytes 2097168 | tf_op jit(solution)/shard_map/all_gather | solution.py:152
  477.7 32.1 %while.15 = (s32[]{:T(128)}, f32[3,2,256,256]{3,2,1,0:T(8,128)S(1)}, f32[2,3,128,2,256]{2,4,3,1,0:T(8,128)}, f32[2]{0:T(128)}, f32[2,3,128,2,256]{2,0,4,3,1:T(2,...) while((s32[]{:T(128)}, ...), condition=%wide.region_6.7_spmd.clone.clone.clone, body=%wide.region_5.6_spmd.clone.clone.clone.sunk | while | flops 1814266368 | bytes 24476680 | solution.py:67
  516.7 45.7 %all-gather.30.cloned.1.call-done = bf16[512,2048]{1,0:T(8,128)(2,1)} async-done(((bf16[512,256]{1,0:T(8,128)(2,1)}), bf16[512,2048]{1,0:T(8,128)(2,1)}) %all-gather.30.cloned.1.call-update) | async-done | bytes 2097168 | tf_op jit(solution)/shard_map/all_gather | solution.py:168
  562.5 8.9 %convolution_convert_fusion = bf16[768,2048]{1,0:T(8,128)(2,1)} fusion(bf16[512,2048]{1,0:T(8,128)(2,1)} %all-gather.30.cloned.1.call-done, f32[768,512]{1,0:T(8,128)} %bitcast.106, f32[768,512]{1,0:T(8,128)S(1)} %bitcast.105, bf16[768,2048]{1,0:T(8,128)(2,1)} %all-gather.20.cloned.1.call-done, bf16[2048,512]{1,0:T(8,128)(2,1)} %all-gather.28.cloned.1.call-done, ...), kind=kOutput, calls=%fused_computation.29 | convolution fusion | flops 3227123712 | bytes 13635584 | tf_op jit(solution)/shard_map/dot_general | solution.py:166
  571.5 36.0 %reduce-scatter.6.cloned.1.call-done = bf16[768,512]{1,0:T(8,128)(2,1)} async-done(((bf16[768,2048]{1,0:T(8,128)(2,1)}), bf16[768,512]{1,0:T(8,128)(2,1)}) %reduce-scatter.6.cloned.1.call-update) | async-done | bytes 786448 | tf_op jit(solution)/shard_map/reduce_scatter | solution.py:84
  609.0 5.8 psum.23
  616.0 29.2 %all-gather.32.cloned.1.call-done = bf16[768,2048]{1,0:T(8,128)(2,1)} async-done(((bf16[768,512]{1,0:T(8,128)(2,1)}), bf16[768,2048]{1,0:T(8,128)(2,1)}) %all-gather.32.cloned.1.call-update) | async-done | bytes 3145744 | tf_op jit(solution)/shard_map/all_gather | solution.py:79
  645.3 6.8 fusion.61
  652.1 11.8 %convolution_convert_fusion.1 = bf16[768,2048]{1,0:T(8,128)(2,1)} fusion(bf16[768,2048]{1,0:T(8,128)(2,1)} %all-gather.18.cloned.1.call-done, f32[768,768]{1,0:T(8,128)} %fusion.61, bf16[768,2048]{1,0:T(8,128)(2,1)} %all-gather.32.cloned.1.call-done, bf16[2048,768]{1,0:T(8,128)(2,1)} %all-gather.16.cloned.1.call-done, f32[768]{0:T(1024)S(1)} %copy-done.30, ...), kind=kOutput, calls=%fused_computation.30 | convolution fusion | flops 4838129664 | bytes 14948352 | tf_op jit(solution)/shard_map/dot_general | solution.py:101
  663.9 37.9 %reduce-scatter.8.cloned.1.call-done = bf16[768,512]{1,0:T(8,128)(2,1)} async-done(((bf16[768,2048]{1,0:T(8,128)(2,1)}), bf16[768,512]{1,0:T(8,128)(2,1)}) %reduce-scatter.8.cloned.1.call-update) | async-done | bytes 786448 | tf_op jit(solution)/shard_map/reduce_scatter | solution.py:84
  (197 shorter events, 119.3 us)
Async XLA Ops:
  6.5 41.1 %all-gather.12.cloned.1.call-start = ((), (), s32[]{:S(2)}) async-start(), calls=%async_computation.3 | async-start | bytes 3932160 | tf_op jit(solution)/shard_map/all_gather | solution.py:79
  18.7 91.2 %all-gather.14.cloned.1.call-start = ((), (), s32[]{:S(2)}) async-start(), calls=%async_computation.4 | async-start | bytes 3538944 | tf_op jit(solution)/shard_map/all_gather | solution.py:92
  19.5 151.2 %all-gather.16.cloned.1.call-start = ((), (), s32[]{:S(2)}) async-start(), calls=%async_computation.5 | async-start | bytes 3538944 | tf_op jit(solution)/shard_map/all_gather | solution.py:97
  20.7 213.3 %all-gather.18.cloned.1.call-start = ((), (), s32[]{:S(2)}) async-start(), calls=%async_computation.6 | async-start | bytes 3538944 | tf_op jit(solution)/shard_map/all_gather | solution.py:103
  21.6 212.4 %copy-start.29 = (f32[768]{0:T(1024)S(1)}, f32[768]{0:T(1024)}, u32[]{:S(2)}) copy-start(f32[768]{0:T(1024)} %param.30) | copy-start | bytes 9220
  21.6 212.4 %copy-start.31 = (f32[768]{0:T(1024)S(1)}, f32[768]{0:T(1024)}, u32[]{:S(2)}) copy-start(f32[768]{0:T(1024)} %param.29) | copy-start | bytes 9220
  21.6 259.5 %reduce-scatter.4.cloned.1.call-start = ((), (), s32[]{:S(2)}) async-start(), calls=%async_computation.7 | async-start | bytes 3932160 | tf_op jit(solution)/shard_map/reduce_scatter | solution.py:84
  47.6 186.4 %copy-start.28 = (bf16[768,2048]{1,0:T(8,128)(2,1)S(1)}, bf16[768,2048]{1,0:T(8,128)(2,1)}, u32[]{:S(2)}) copy-start(bf16[768,2048]{1,0:T(8,128)(2,1)} %all-gather.12.cloned.1.call-done) | copy-start | bytes 9437188
  245.1 43.5 %copy-start.24 = (f32[512]{0:T(512)S(1)}, f32[512]{0:T(512)}, u32[]{:S(2)}) copy-start(f32[512]{0:T(512)} %param.32) | copy-start | bytes 6148
  245.1 87.2 %all-gather.26.cloned.1.call-start = ((), (), s32[]{:S(2)}) async-start(), calls=%async_computation.11 | async-start | bytes 2359296 | tf_op jit(solution)/shard_map/all_gather | solution.py:150
  246.8 114.0 %all-gather.20.cloned.1.call-start = ((), (), s32[]{:S(2)}) async-start(), calls=%async_computation.8 | async-start | bytes 3932160 | tf_op jit(solution)/shard_map/all_gather | solution.py:79
  246.9 41.7 %copy-start.19 = (f32[512]{0:T(512)}, f32[512]{0:T(512)S(1)}, u32[]{:S(2)}) copy-start(f32[512]{0:T(512)S(1)} %broadcast_multiply_fusion.1) | copy-start | bytes 6148
  289.8 122.3 %all-gather.22.cloned.1.call-start = ((), (), s32[]{:S(2)}) async-start(), calls=%async_computation.9 | async-start | bytes 2359296 | tf_op jit(solution)/shard_map/all_gather | solution.py:151
  290.6 171.3 %all-gather.24.cloned.1.call-start = ((), (), s32[]{:S(2)}) async-start(), calls=%async_computation.10 | async-start | bytes 2359296 | tf_op jit(solution)/shard_map/all_gather | solution.py:152
  291.4 69.4 %copy-start.33 = (f32[512]{0:T(512)S(1)}, f32[512]{0:T(512)}, u32[]{:S(2)}) copy-start(f32[512]{0:T(512)} %param.37) | copy-start | bytes 6148
  291.5 225.3 %all-gather.28.cloned.1.call-start = ((), (), s32[]{:S(2)}) async-start(), calls=%async_computation.12 | async-start | bytes 2359296 | tf_op jit(solution)/shard_map/all_gather | solution.py:153
  292.3 270.2 %all-gather.30.cloned.1.call-start = ((), (), s32[]{:S(2)}) async-start(), calls=%async_computation.13 | async-start | bytes 2359296 | tf_op jit(solution)/shard_map/all_gather | solution.py:168
  293.1 314.4 %reduce-scatter.6.cloned.1.call-start = ((), (), s32[]{:S(2)}) async-start(), calls=%async_computation.14 | async-start | bytes 3932160 | tf_op jit(solution)/shard_map/reduce_scatter | solution.py:84
  366.9 45.2 %copy-start.34 = (f32[512]{0:T(512)S(1)}, f32[512]{0:T(512)}, u32[]{:S(2)}) copy-start(f32[512]{0:T(512)} %param.38) | copy-start | bytes 6148
  515.4 47.1 %copy-start.36 = (f32[512]{0:T(512)S(1)}, f32[512]{0:T(512)}, u32[]{:S(2)}) copy-start(f32[512]{0:T(512)} %param.40) | copy-start | bytes 6148
  515.4 47.0 %copy-start.37 = (f32[512]{0:T(512)S(1)}, f32[512]{0:T(512)}, u32[]{:S(2)}) copy-start(f32[512]{0:T(512)} %param.41) | copy-start | bytes 6148
  571.5 43.3 %copy-start.25 = (f32[512]{0:T(512)S(1)}, f32[512]{0:T(512)}, u32[]{:S(2)}) copy-start(f32[512]{0:T(512)} %param.45) | copy-start | bytes 6148
  571.5 73.8 %all-gather.32.cloned.1.call-start = ((), (), s32[]{:S(2)}) async-start(), calls=%async_computation.15 | async-start | bytes 3932160 | tf_op jit(solution)/shard_map/all_gather | solution.py:79
  616.0 85.8 %reduce-scatter.8.cloned.1.call-start = ((), (), s32[]{:S(2)}) async-start(), calls=%async_computation.16 | async-start | bytes 3932160 | tf_op jit(solution)/shard_map/reduce_scatter | solution.py:84
  (38 other events, 324.2 us)
Sparse Core Ops, SparseCore 0:
  18.8 28.8 all-gather.11
  49.8 60.0 all-gather.13
  112.1 58.6 all-gather.15
  172.7 61.3 all-gather.17
  245.2 35.8 reduce-scatter.3
  283.1 49.1 all-gather.25
  333.8 27.0 all-gather.19
  363.0 49.0 all-gather.21
  414.2 47.6 all-gather.23
  463.9 47.6 all-gather.27
  513.6 48.8 all-gather.29
  571.6 35.8 reduce-scatter.5
  616.1 29.1 all-gather.31
  664.1 37.7 reduce-scatter.7
where the time goes:
time: 718 us; the launch traced here: 711 us
  waiting for transfers between devices  498 us (69%)
  matrix products  81.8 us (11%)
  local copies, waits for them, and re-layouts  52.8 us (7%)
  other arithmetic  43.2 us (6%)
  blocking collectives  20 us (3%)
  between operations  13.9 us (2%)
    reduce_scatter x3, waiting for transfers between devices, summed_share(): lax.psum_scatter(rounded.astype(jnp.float32).astype(jnp.bfloat16), 'tp',...  108 us
    all_gather x3, waiting for transfers between devices, normed_rows(): return lax.all_gather(scaled.astype(jnp.bfloat16), 'tp', axis=1, tiled=True)  83.8 us
    all_gather x1, waiting for transfers between devices, ffn_gathered(): lax.all_gather(down_low, 'fs', axis=1, tiled=True)  63.2 us
    all_gather x1, waiting for transfers between devices, ffn_gathered(): lax.all_gather(gate_low, 'fs', axis=0, tiled=True)  62.2 us
    all_gather x1, waiting for transfers between devices, ffn_gathered(): lax.all_gather(up_low, 'fs', axis=0, tiled=True)  54.1 us
    all_gather x1, waiting for transfers between devices, per_device(): lax.all_gather(w_mix.astype(jnp.bfloat16), 'fs', axis=1, tiled=True)  45.7 us
    all_gather x1, waiting for transfers between devices, per_device(): lax.all_gather(w_key.astype(jnp.bfloat16), 'fs', axis=0, tiled=True)  43 us
    all_gather x1, waiting for transfers between devices, per_device(): lax.all_gather(w_query.astype(jnp.bfloat16), 'fs', axis=0, tiled=True)  28.7 us
  transfers between devices with their start and end apart: 14, of which 13 were waited for; matrix products, arithmetic and copies ran while one was open for 18% of the time, Pallas kernels for 0%

commit v1 on v0

--- a/solution.py
+++ b/solution.py
@@ -76,7 +76,7 @@
     widened = hidden_in.astype(jnp.float32)
     totals = lax.psum(jnp.sum(widened * widened, axis=1), "tp")
     scaled = widened * lax.rsqrt(totals / D + EPS)[:, None] * norm_gain
-    return lax.all_gather(scaled.astype(jnp.bfloat16), "tp", axis=1, tiled=True)
+    return jnp.concatenate(lax.all_gather(scaled.astype(jnp.bfloat16), "tp"), axis=1)
 
 
 def summed_share(partial_value):

time: 718 us -> 733 us (1.021)
  local copies, waits for them, and re-layouts: 52.8 us -> 79.7 us
  waiting for transfers between devices: 498 us -> 485 us
    all_gather x1, waiting for transfers between devices: 28.7 us -> 46.6 us  [per_device(): lax.all_gather(w_query.astype(jnp.bfloat16), 'fs', axis=0, tiled=True)]
    all_gather x3, waiting for transfers between devices: 83.8 us -> 70.2 us  [normed_rows(): lax.all_gather(scaled.astype(jnp.bfloat16), 'tp')]
    all_gather x0 -> x3, local copies, waits for them, and re-layouts: none -> 12.6 us  [normed_rows(): lax.all_gather(scaled.astype(jnp.bfloat16), 'tp')]
    reshape x4, local copies, waits for them, and re-layouts: 15.1 us -> 24.3 us  [split_heads(): values.astype(jnp.float32).reshape(sequences, length, heads, head_size)]
    all_gather x1, waiting for transfers between devices: 8.76 us -> 0.02 us  [per_device(): lax.all_gather(w_value.astype(jnp.bfloat16), 'fs', axis=0, tiled=True)]
  transfers between devices with their start and end apart: 14 -> 14, of which waited for: 13 -> 12; matrix products, arithmetic and copies ran while one was open for 18% -> 20% of each run, Pallas kernels for 0% -> 0%
where the time goes in v1:
time: 733 us; the launch traced here: 724 us
  waiting for transfers between devices  485 us (66%)
  matrix products  80.7 us (11%)
  local copies, waits for them, and re-layouts  79.7 us (11%)
  other arithmetic  43.4 us (6%)
  blocking collectives  20 us (3%)
  between operations  14 us (2%)
    reduce_scatter x3, waiting for transfers between devices, summed_share(): lax.psum_scatter(rounded.astype(jnp.float32).astype(jnp.bfloat16), 'tp',...  109 us
    all_gather x3, waiting for transfers between devices, normed_rows(): lax.all_gather(scaled.astype(jnp.bfloat16), 'tp')  70.2 us
    all_gather x1, waiting for transfers between devices, ffn_gathered(): lax.all_gather(down_low, 'fs', axis=1, tiled=True)  63.2 us
    all_gather x1, waiting for transfers between devices, ffn_gathered(): lax.all_gather(gate_low, 'fs', axis=0, tiled=True)  59 us
    all_gather x1, waiting for transfers between devices, ffn_gathered(): lax.all_gather(up_low, 'fs', axis=0, tiled=True)  54.9 us
    all_gather x1, waiting for transfers between devices, per_device(): lax.all_gather(w_query.astype(jnp.bfloat16), 'fs', axis=0, tiled=True)  46.6 us
    all_gather x1, waiting for transfers between devices, per_device(): lax.all_gather(w_key.astype(jnp.bfloat16), 'fs', axis=0, tiled=True)  41.6 us
    all_gather x1, waiting for transfers between devices, per_device(): lax.all_gather(w_mix.astype(jnp.bfloat16), 'fs', axis=1, tiled=True)  40.4 us
  transfers between devices with their start and end apart: 14, of which 12 were waited for; matrix products, arithmetic and copies ran while one was open for 20% of the time, Pallas kernels for 0%

profile of v1, /device:TPU:0, one launch (start us, length us, event | category | flops | bytes accessed | tf_op | source)
XLA Modules:
  0.0 724.0 jit_solution(8532640827104849418)
XLA Ops:
  8.0 8.4 %psum.21 = f32[768]{0:T(1024)S(1)} all-reduce(f32[768]{0:T(1024)S(1)} %fusion.31), channel_id=1, replica_groups=mesh['fs'=8,'tp'=4] {'tp'}, use_global_device_ids=true, to_apply=%region_1.0 | all-reduce | flops 768 | bytes 6144 | tf_op jit(solution)/shard_map/psum | solution.py:77
  21.6 26.0 %all-gather.31.cloned.1.call-done = bf16[3072,512]{1,0:T(8,128)(2,1)} async-done(((bf16[768,512]{1,0:T(8,128)(2,1)}), bf16[3072,512]{1,0:T(8,128)(2,1)}) %all-gather.31.cloned.1.call-update) | async-done | bytes 3145744 | tf_op jit(solution)/shard_map/all_gather | solution.py:79
  50.8 59.0 %all-gather.15.cloned.1.call-done = bf16[2048,768]{1,0:T(8,128)(2,1)} async-done(((bf16[256,768]{1,0:T(8,128)(2,1)}), bf16[2048,768]{1,0:T(8,128)(2,1)}) %all-gather.15.cloned.1.call-update) | async-done | bytes 3145744 | tf_op jit(solution)/shard_map/all_gather | solution.py:92
  109.9 6.0 fusion.60
  115.9 54.9 %all-gather.17.cloned.1.call-done = bf16[2048,768]{1,0:T(8,128)(2,1)} async-done(((bf16[256,768]{1,0:T(8,128)(2,1)}), bf16[2048,768]{1,0:T(8,128)(2,1)}) %all-gather.17.cloned.1.call-update) | async-done | bytes 3145744 | tf_op jit(solution)/shard_map/all_gather | solution.py:97
  170.8 63.2 %all-gather.19.cloned.1.call-done = bf16[768,2048]{1,0:T(8,128)(2,1)} async-done(((bf16[768,256]{1,0:T(8,128)(2,1)}), bf16[768,2048]{1,0:T(8,128)(2,1)}) %all-gather.19.cloned.1.call-update) | async-done | bytes 3145744 | tf_op jit(solution)/shard_map/all_gather | solution.py:103
  234.0 11.4 %convolution_convert_fusion.2 = bf16[768,2048]{1,0:T(8,128)(2,1)} fusion(bf16[768,2048]{1,0:T(8,128)(2,1)} %all-gather.19.cloned.1.call-done, f32[768,768]{1,0:T(8,128)} %fusion.60, bf16[768,2048]{0,1:T(8,128)(2,1)S(1)} %bitcast.124, bf16[2048,768]{1,0:T(8,128)(2,1)} %all-gather.17.cloned.1.call-done, f32[768]{0:T(1024)S(1)} %copy-done.32, ...), kind=kOutput, calls=%fused_computation.31 | convolution fusion | flops 4838129664 | bytes 14948352 | tf_op jit(solution)/shard_map/dot_general | solution.py:101
  246.1 35.4 %reduce-scatter.4.cloned.1.call-done = bf16[768,512]{1,0:T(8,128)(2,1)} async-done(((bf16[768,2048]{1,0:T(8,128)(2,1)}), bf16[768,512]{1,0:T(8,128)(2,1)}) %reduce-scatter.4.cloned.1.call-update) | async-done | bytes 786448 | tf_op jit(solution)/shard_map/reduce_scatter | solution.py:84
  283.0 5.9 psum.22
  295.9 8.6 %multiply_cosine_fusion = (f32[2,128,256]{1,0,2:T(2,128)S(1)}, f32[2,128,256]{1,0,2:T(2,128)}, f32[2,128,256]{1,0,2:T(2,128)}) fusion(f32[2,128]{1,0:T(2,128)S(1)} %multiply_add_fusion.1, f32[256]{0:T(256)S(1)} %mul.404), kind=kLoop, calls=%fused_computation.82 | loop fusion | flops 327680 | bytes 788480 | tf_op jit(solution)/shard_map/cos | solution.py:33
  304.5 14.9 %all-gather.33.cloned.1.call-done = bf16[3072,512]{1,0:T(8,128)(2,1)} async-done(((bf16[768,512]{1,0:T(8,128)(2,1)}), bf16[3072,512]{1,0:T(8,128)(2,1)}) %all-gather.33.cloned.1.call-update) | async-done | bytes 3145744 | tf_op jit(solution)/shard_map/all_gather | solution.py:79
  324.1 46.6 %all-gather.25.cloned.1.call-done = bf16[2048,512]{1,0:T(8,128)(2,1)} async-done(((bf16[256,512]{1,0:T(8,128)(2,1)}), bf16[2048,512]{1,0:T(8,128)(2,1)}) %all-gather.25.cloned.1.call-update) | async-done | bytes 2097168 | tf_op jit(solution)/shard_map/all_gather | solution.py:150
  378.9 41.6 %all-gather.21.cloned.1.call-done = bf16[2048,512]{1,0:T(8,128)(2,1)} async-done(((bf16[256,512]{1,0:T(8,128)(2,1)}), bf16[2048,512]{1,0:T(8,128)(2,1)}) %all-gather.21.cloned.1.call-update) | async-done | bytes 2097168 | tf_op jit(solution)/shard_map/all_gather | solution.py:151
  420.5 5.5 broadcast_multiply_fusion
  457.6 14.3 %copy.70 = f32[3,2,128,2,256]{2,1,4,3,0:T(2,128)} copy(f32[3,2,128,2,256]{4,3,2,1,0:T(2,128)} %reshape.177) | data formatting | bytes 3145728 | tf_op jit(solution)/shard_map/reshape | solution.py:27
  487.8 31.9 %while.15 = (s32[]{:T(128)}, f32[3,2,256,256]{3,2,1,0:T(8,128)S(1)}, f32[2,3,128,2,256]{2,4,3,1,0:T(8,128)}, f32[2]{0:T(128)}, f32[2,3,128,2,256]{2,0,4,3,1:T(2,...) while((s32[]{:T(128)}, ...), condition=%wide.region_6.7_spmd.clone.clone.clone, body=%wide.region_5.6_spmd.clone.clone.clone.sunk | while | flops 1814266368 | bytes 24476680 | solution.py:67
  530.5 40.4 %all-gather.29.cloned.1.call-done = bf16[512,2048]{1,0:T(8,128)(2,1)} async-done(((bf16[512,256]{1,0:T(8,128)(2,1)}), bf16[512,2048]{1,0:T(8,128)(2,1)}) %all-gather.29.cloned.1.call-update) | async-done | bytes 2097168 | tf_op jit(solution)/shard_map/all_gather | solution.py:168
  570.8 8.6 %convolution_convert_fusion = bf16[768,2048]{1,0:T(8,128)(2,1)} fusion(bf16[512,2048]{1,0:T(8,128)(2,1)} %all-gather.29.cloned.1.call-done, f32[768,512]{1,0:T(8,128)} %bitcast.129, f32[768,512]{1,0:T(8,128)} %bitcast.128, bf16[768,2048]{0,1:T(8,128)(2,1)S(1)} %bitcast.118, bf16[2048,512]{1,0:T(8,128)(2,1)} %all-gather.27.cloned.1.call-done, ...), kind=kOutput, calls=%fused_computation.29 | convolution fusion | flops 3227123712 | bytes 13635584 | tf_op jit(solution)/shard_map/dot_general | solution.py:166
  579.5 36.0 %reduce-scatter.6.cloned.1.call-done = bf16[768,512]{1,0:T(8,128)(2,1)} async-done(((bf16[768,2048]{1,0:T(8,128)(2,1)}), bf16[768,512]{1,0:T(8,128)(2,1)}) %reduce-scatter.6.cloned.1.call-update) | async-done | bytes 786448 | tf_op jit(solution)/shard_map/reduce_scatter | solution.py:84
  617.0 5.8 psum.23
  624.0 29.2 %all-gather.35.cloned.1.call-done = bf16[3072,512]{1,0:T(8,128)(2,1)} async-done(((bf16[768,512]{1,0:T(8,128)(2,1)}), bf16[3072,512]{1,0:T(8,128)(2,1)}) %all-gather.35.cloned.1.call-update) | async-done | bytes 3145744 | tf_op jit(solution)/shard_map/all_gather | solution.py:79
  657.9 6.9 fusion.61
  664.9 12.1 %convolution_convert_fusion.1 = bf16[768,2048]{1,0:T(8,128)(2,1)} fusion(bf16[768,2048]{1,0:T(8,128)(2,1)} %all-gather.19.cloned.1.call-done, f32[768,768]{1,0:T(8,128)} %fusion.61, bf16[768,2048]{0,1:T(8,128)(2,1)} %bitcast.127, bf16[2048,768]{1,0:T(8,128)(2,1)} %all-gather.17.cloned.1.call-done, f32[768]{0:T(1024)S(1)} %copy-done.33, f32[768]{0:T(1024)S(1)} %copy-done.35), kind=kOutput, calls=%fused_computation.30 | convolution fusion | flops 4838129664 | bytes 14948352 | tf_op jit(solution)/shard_map/dot_general | solution.py:101
  677.0 37.9 %reduce-scatter.8.cloned.1.call-done = bf16[768,512]{1,0:T(8,128)(2,1)} async-done(((bf16[768,2048]{1,0:T(8,128)(2,1)}), bf16[768,512]{1,0:T(8,128)(2,1)}) %reduce-scatter.8.cloned.1.call-update) | async-done | bytes 786448 | tf_op jit(solution)/shard_map/reduce_scatter | solution.py:84
  (200 shorter events, 131.2 us)
Async XLA Ops:
  6.5 41.1 %all-gather.31.cloned.1.call-start = ((), (), s32[]{:S(2)}) async-start(), calls=%async_computation.14 | async-start | bytes 3932160 | tf_op jit(solution)/shard_map/all_gather | solution.py:79
  18.7 91.2 %all-gather.15.cloned.1.call-start = ((), (), s32[]{:S(2)}) async-start(), calls=%async_computation.3 | async-start | bytes 3538944 | tf_op jit(solution)/shard_map/all_gather | solution.py:92
  19.5 151.2 %all-gather.17.cloned.1.call-start = ((), (), s32[]{:S(2)}) async-start(), calls=%async_computation.4 | async-start | bytes 3538944 | tf_op jit(solution)/shard_map/all_gather | solution.py:97
  20.7 213.3 %all-gather.19.cloned.1.call-start = ((), (), s32[]{:S(2)}) async-start(), calls=%async_computation.5 | async-start | bytes 3538944 | tf_op jit(solution)/shard_map/all_gather | solution.py:103
  21.6 259.9 %reduce-scatter.4.cloned.1.call-start = ((), (), s32[]{:S(2)}) async-start(), calls=%async_computation.6 | async-start | bytes 3932160 | tf_op jit(solution)/shard_map/reduce_scatter | solution.py:84
  109.9 124.2 %copy-start.32 = (f32[768]{0:T(1024)S(1)}, f32[768]{0:T(1024)}, u32[]{:S(2)}) copy-start(f32[768]{0:T(1024)} %param.30) | copy-start | bytes 9220
  109.9 124.2 %copy-start.34 = (f32[768]{0:T(1024)S(1)}, f32[768]{0:T(1024)}, u32[]{:S(2)}) copy-start(f32[768]{0:T(1024)} %param.29) | copy-start | bytes 9220
  245.4 43.5 %copy-start.28 = (f32[512]{0:T(512)S(1)}, f32[512]{0:T(512)}, u32[]{:S(2)}) copy-start(f32[512]{0:T(512)} %param.32) | copy-start | bytes 6148
  245.4 74.0 %all-gather.33.cloned.1.call-start = ((), (), s32[]{:S(2)}) async-start(), calls=%async_computation.15 | async-start | bytes 3932160 | tf_op jit(solution)/shard_map/all_gather | solution.py:79
  246.1 42.9 %copy-start.23 = (f32[512]{0:T(512)}, f32[512]{0:T(512)S(1)}, u32[]{:S(2)}) copy-start(f32[512]{0:T(512)S(1)} %broadcast_multiply_fusion.1) | copy-start | bytes 6148
  290.1 80.5 %all-gather.25.cloned.1.call-start = ((), (), s32[]{:S(2)}) async-start(), calls=%async_computation.9 | async-start | bytes 2359296 | tf_op jit(solution)/shard_map/all_gather | solution.py:150
  291.0 129.5 %all-gather.21.cloned.1.call-start = ((), (), s32[]{:S(2)}) async-start(), calls=%async_computation.7 | async-start | bytes 2359296 | tf_op jit(solution)/shard_map/all_gather | solution.py:151
  291.8 180.2 %all-gather.23.cloned.1.call-start = ((), (), s32[]{:S(2)}) async-start(), calls=%async_computation.8 | async-start | bytes 2359296 | tf_op jit(solution)/shard_map/all_gather | solution.py:152
  292.7 237.8 %all-gather.27.cloned.1.call-start = ((), (), s32[]{:S(2)}) async-start(), calls=%async_computation.10 | async-start | bytes 2359296 | tf_op jit(solution)/shard_map/all_gather | solution.py:153
  293.5 277.3 %all-gather.29.cloned.1.call-start = ((), (), s32[]{:S(2)}) async-start(), calls=%async_computation.11 | async-start | bytes 2359296 | tf_op jit(solution)/shard_map/all_gather | solution.py:168
  294.3 321.2 %reduce-scatter.6.cloned.1.call-start = ((), (), s32[]{:S(2)}) async-start(), calls=%async_computation.12 | async-start | bytes 3932160 | tf_op jit(solution)/shard_map/reduce_scatter | solution.py:84
  319.4 51.3 %copy-start.18 = (f32[512]{0:T(512)S(1)}, f32[512]{0:T(512)}, u32[]{:S(2)}) copy-start(f32[512]{0:T(512)} %param.37) | copy-start | bytes 6148
  376.7 43.7 %copy-start.19 = (f32[512]{0:T(512)S(1)}, f32[512]{0:T(512)}, u32[]{:S(2)}) copy-start(f32[512]{0:T(512)} %param.38) | copy-start | bytes 6148
  523.7 47.2 %copy-start.37 = (f32[512]{0:T(512)S(1)}, f32[512]{0:T(512)}, u32[]{:S(2)}) copy-start(f32[512]{0:T(512)} %param.41) | copy-start | bytes 6148
  527.6 43.3 %copy-start.1 = (bf16[4,768,512]{1,2,0:T(8,128)(2,1)S(1)}, bf16[4,768,512]{1,2,0:T(8,128)(2,1)}, u32[]{:S(2)}) copy-start(bf16[4,768,512]{1,2,0:T(8,128)(2,1)} %copy.65) | copy-start | bytes 9437188
  527.6 43.3 %copy-start.36 = (f32[512]{0:T(512)S(1)}, f32[512]{0:T(512)}, u32[]{:S(2)}) copy-start(f32[512]{0:T(512)} %param.40) | copy-start | bytes 6148
  579.4 43.4 %copy-start.29 = (f32[512]{0:T(512)S(1)}, f32[512]{0:T(512)}, u32[]{:S(2)}) copy-start(f32[512]{0:T(512)} %param.45) | copy-start | bytes 6148
  579.4 73.8 %all-gather.35.cloned.1.call-start = ((), (), s32[]{:S(2)}) async-start(), calls=%async_computation.16 | async-start | bytes 3932160 | tf_op jit(solution)/shard_map/all_gather | solution.py:79
  624.0 90.9 %reduce-scatter.8.cloned.1.call-start = ((), (), s32[]{:S(2)}) async-start(), calls=%async_computation.13 | async-start | bytes 3932160 | tf_op jit(solution)/shard_map/reduce_scatter | solution.py:84
  (38 other events, 266.1 us)
Sparse Core Ops, SparseCore 0:
  18.8 28.8 all-gather.30
  49.8 60.0 all-gather.14
  112.1 58.6 all-gather.16
  172.7 61.3 all-gather.18
  245.5 35.8 reduce-scatter.3
  290.2 29.1 all-gather.32
  321.5 49.0 all-gather.24
  372.8 47.6 all-gather.20
  422.6 47.5 all-gather.22
  472.2 47.6 all-gather.26
  521.9 48.8 all-gather.28
  579.5 35.8 reduce-scatter.5
  624.1 29.1 all-gather.34
  677.1 37.7 reduce-scatter.7
